TPU v7x, 32 devices: a whole 2x2x4 slice. The times are simulated.
32 devices in a mesh: sp: 8 (over z, y), tp: 4 (over x, core).
Axes of the slice: x: 2, y: 2, z: 4, core: 2. Of those that a mesh axis runs over, the one named last changes fastest.
Arguments:
- residual: bfloat16 [2048, 2048], P(('sp', 'tp')), may hold values from -6 to 6
- queries: bfloat16 [2048, 2048], P('sp', 'tp'), may hold values from -40 to 40
- key_rows: bfloat16 [2048, 1024], P('sp', 'tp'), may hold values from -40 to 40
- value_rows: bfloat16 [2048, 1024], P('sp', 'tp'), may hold values from -6 to 6
- forget_sums: float32 [2048, 16], P('sp', 'tp'), as said below
- out_weight: bfloat16 [2048, 2048], P('tp'), may hold values from -0.25 to 0.25
- norm_gain: float32 [2048], replicated, may hold values from 0.1 to 1.9
- expert_ids: int32 [2048, 4], P(('sp', 'tp')), may hold values from 0 to 7, all different within a row; in each aligned block of 64 rows (0 to 63, 64 to 127, ...) at most 64 rows name the same one
- route_weights: float32 [2048, 4], P(('sp', 'tp')), may hold values from 0.1 to 1
- expert_gate: bfloat16 [8, 2048, 384], P('sp'), may hold values from -0.125 to 0.125
- expert_up: bfloat16 [8, 2048, 384], P('sp'), may hold values from -0.125 to 0.125
- expert_down: bfloat16 [8, 384, 2048], P('sp'), may hold values from -0.3125 to 0.3125
- shared_gate: bfloat16 [2048, 384], replicated, may hold values from -0.125 to 0.125
- shared_up: bfloat16 [2048, 384], replicated, may hold values from -0.125 to 0.125
- shared_down: bfloat16 [384, 2048], replicated, may hold values from -0.3125 to 0.3125
Outputs:
- layer_out: bfloat16 [2048, 2048], P(('sp', 'tp'))
Inputs may be any that keep to these rules, and one draw needn't show every extreme that they name: `forget_sums`: each head's column never rises from one position to the next. `expert_ids`: each row names 4 different experts; among the rows of one device no expert is named more than 64 times.
All inputs are finite; a program needn't handle non-finite values.
Results may differ from a plain program's by a relative error of at most 0.014.
Values may be sent and summed in bfloat16 or wider, within the bound.
A program may use at most 128 MiB of HBM per device.

v0:
```python
import math
import jax
import jax.numpy as jnp
from jax import lax
from jax.sharding import PartitionSpec as P

HEADS = 16
KV_HEADS = 8
HEAD_DIM = 128
TOPK = 4
routed_scale = 2.5
norm_eps = 1e-06


def absorb_group(carried, query_group, shard_piece, sum_piece, score_scale):
    query_heads, query_sums, query_pos, last_pos = query_group
    key_piece, value_piece = shard_piece
    piece_rows = key_piece.shape[0]
    query_count, local_kv, group_size, head_size = query_heads.shape
    key_block = math.gcd(piece_rows, 1024)
    key_heads = key_piece.reshape(piece_rows, local_kv, head_size)
    value_heads = value_piece.reshape(piece_rows, local_kv, head_size)
    key_sums = sum_piece.reshape(piece_rows, local_kv, group_size).transpose(1, 2, 0)

    def update(block_start, held):
        row_max, row_sum, weighted = held
        key_part = lax.dynamic_slice_in_dim(key_heads, block_start, key_block, 0)
        value_part = lax.dynamic_slice_in_dim(value_heads, block_start, key_block, 0)
        sums_part = lax.dynamic_slice_in_dim(key_sums, block_start, key_block, 2)
        scores = (
            jnp.einsum("qhgd,khd->hgqk", query_heads, key_part, preferred_element_type=jnp.float32)
            * score_scale
        )
        scores = scores + (query_sums[:, :, :, None] - sums_part[:, :, None, :])
        key_pos = block_start + jnp.arange(key_block, dtype=jnp.int32)
        allowed = query_pos[:, None] >= key_pos[None, :]
        scores = jnp.where(allowed, scores, -jnp.inf)
        new_max = jnp.maximum(row_max, jnp.max(scores, axis=3))
        weights = jnp.exp(scores - new_max[:, :, :, None])
        factor = jnp.exp(row_max - new_max)
        row_sum = row_sum * factor + jnp.sum(weights, axis=3)
        products = jnp.einsum(
            "hgqk,khd->qhgd",
            weights.astype(jnp.bfloat16),
            value_part,
            preferred_element_type=jnp.float32,
        )
        weighted = weighted * factor.transpose(2, 0, 1)[:, :, :, None] + products
        return (new_max, row_sum, weighted)

    def one_block(block_index, held):
        block_start = block_index * key_block
        needed = block_start <= last_pos
        return lax.cond(needed, lambda inner: update(block_start, inner), lambda inner: inner, held)

    return lax.fori_loop(0, piece_rows // key_block, one_block, carried)


def finish(carried):
    row_max, row_sum, weighted = carried
    mixed = weighted / row_sum.transpose(2, 0, 1)[:, :, :, None]
    return mixed.reshape(mixed.shape[0], -1).astype(jnp.bfloat16)


def local(
    residual,
    queries,
    key_rows,
    value_rows,
    forget_sums,
    out_weight,
    norm_gain,
    expert_ids,
    route_weights,
    expert_gate,
    expert_up,
    expert_down,
    shared_gate,
    shared_up,
    shared_down,
):
    sp_count = lax.axis_size("sp")
    sp_index = lax.axis_index("sp")
    local_rows = queries.shape[0]
    local_kv = key_rows.shape[1] // HEAD_DIM
    group_size = HEADS // KV_HEADS
    score_scale = HEAD_DIM ** (-0.5)
    own_first = sp_index * local_rows
    all_sums = lax.all_gather(forget_sums, "sp", axis=0, tiled=True)
    positions = own_first + jnp.arange(local_rows, dtype=jnp.int32)
    groups = [
        (
            queries.reshape(queries.shape[0], local_kv, group_size, HEAD_DIM),
            forget_sums.reshape(forget_sums.shape[0], local_kv, group_size).transpose(1, 2, 0),
            positions,
            positions[-1],
        )
    ]

    def initial(query_count):
        return (
            jnp.full((local_kv, group_size, query_count), -1e30, jnp.float32),
            jnp.zeros((local_kv, group_size, query_count), jnp.float32),
            jnp.zeros((query_count, local_kv, group_size, HEAD_DIM), jnp.float32),
        )

    def absorb(states, shard_piece):
        return tuple(
            (
                absorb_group(held, query_group, shard_piece, all_sums, score_scale)
                for held, query_group in zip(states, groups)
            )
        )

    start_states = tuple((initial(query_group[0].shape[0]) for query_group in groups))
    states = absorb(
        start_states,
        (
            lax.all_gather(key_rows, "sp", axis=0, tiled=True),
            lax.all_gather(value_rows, "sp", axis=0, tiled=True),
        ),
    )
    outputs = [finish(held) for held in states]
    attended = outputs[0]
    rows_out = local_rows // lax.axis_size("tp")
    branch = lax.psum_scatter(
        jnp.dot(attended, out_weight, preferred_element_type=jnp.float32).astype(jnp.bfloat16),
        "tp",
        scatter_dimension=0,
        tiled=True,
    ).astype(jnp.float32)
    stream = (residual.astype(jnp.float32) + branch).astype(jnp.bfloat16)
    wide = lax.optimization_barrier(stream).astype(jnp.float32)
    normed = (
        wide * lax.rsqrt(jnp.mean(wide * wide, axis=1, keepdims=True) + norm_eps) * norm_gain
    ).astype(jnp.bfloat16)
    width = normed.shape[1]
    experts_here = expert_gate.shape[0]
    total_experts = experts_here * sp_count
    capacity = 2 * rows_out * TOPK // total_experts
    flat_ids = expert_ids.reshape(-1)
    assigned = flat_ids.shape[0]
    onehot = (flat_ids[:, None] == jnp.arange(total_experts, dtype=jnp.int32)[None, :]).astype(
        jnp.int32
    )
    slot_rank = jnp.sum((jnp.cumsum(onehot, axis=0) - 1) * onehot, axis=1)
    target = flat_ids * capacity + slot_rank
    slot_count = total_experts * capacity
    source = (
        jnp.full((slot_count,), assigned, jnp.int32)
        .at[target]
        .set(jnp.arange(assigned, dtype=jnp.int32))
    )
    padded = jnp.concatenate([normed, jnp.zeros((1, width), jnp.bfloat16)], axis=0)
    outgoing = padded[source // TOPK].reshape(sp_count, experts_here, capacity, width)
    arrived = lax.all_to_all(outgoing, "sp", split_axis=0, concat_axis=0, tiled=True)
    gate_part = jnp.einsum(
        "necd,edf->necf", arrived, expert_gate, preferred_element_type=jnp.float32
    )
    up_part = jnp.einsum("necd,edf->necf", arrived, expert_up, preferred_element_type=jnp.float32)
    hidden = (jax.nn.silu(gate_part) * up_part).astype(jnp.bfloat16)
    processed = jnp.einsum(
        "necf,efd->necd", hidden, expert_down, preferred_element_type=jnp.float32
    ).astype(jnp.bfloat16)
    returned = lax.all_to_all(processed, "sp", split_axis=0, concat_axis=0, tiled=True)
    results = returned.reshape(slot_count, width)
    picked = results[target].reshape(rows_out, TOPK, width).astype(jnp.float32)
    gates = route_weights / jnp.sum(route_weights, axis=1, keepdims=True) * routed_scale
    routed = jnp.sum(gates[:, :, None] * picked, axis=1)
    shared_hidden = (
        jax.nn.silu(jnp.dot(normed, shared_gate, preferred_element_type=jnp.float32))
        * jnp.dot(normed, shared_up, preferred_element_type=jnp.float32)
    ).astype(jnp.bfloat16)
    shared_out = jnp.dot(shared_hidden, shared_down, preferred_element_type=jnp.float32)
    return (wide + shared_out + routed).astype(jnp.bfloat16)


def solution(mesh):
    in_specs = (
        P(("sp", "tp"), None),
        P("sp", "tp"),
        P("sp", "tp"),
        P("sp", "tp"),
        P("sp", "tp"),
        P("tp", None),
        P(),
        P(("sp", "tp"), None),
        P(("sp", "tp"), None),
        P("sp", None, None),
        P("sp", None, None),
        P("sp", None, None),
        P(),
        P(),
        P(),
    )
    out_specs = P(("sp", "tp"), None)
    return jax.shard_map(local, mesh=mesh, in_specs=in_specs, out_specs=out_specs, check_vma=False)
```

profile of v0, /device:TPU:0, one launch (start us, length us, event | category | flops | bytes accessed | tf_op | source)
XLA Modules:
  0.0 271.7 jit_solution(16404299911886271078)
XLA Ops:
  6.5 1.8 copy.30
  8.4 0.7 all-gather.5.cloned.1.call-update
  9.2 0.6 slice.9
  9.8 1.1 copy.31
  11.1 0.7 reshape.117
  11.8 33.0 %all_gather.10 = f32[2048,4]{0,1:T(4,128)S(1)} all-gather(f32[256,4]{0,1:T(4,128)} %param.23), channel_id=1, replica_groups=mesh['sp'=8,'tp'=4] {'sp'}, dimensions={0}, use_global_device_ids=true | all-gather | bytes 36864 | tf_op jit(solution)/shard_map/all_gather | solution.py:89
  44.8 6.7 %all-gather.3.cloned.1.call-done = bf16[2048,256]{0,1:T(8,128)(2,1)} async-done(((bf16[256,256]{0,1:T(8,128)(2,1)}), bf16[2048,256]{0,1:T(8,128)(2,1)}) %all-gather.3.cloned.1.call-update) | async-done | bytes 1048592 | tf_op jit(solution)/shard_map/all_gather | solution.py:119
  51.5 2.3 copy.33
  53.8 39.2 %all-gather.5.cloned.1.call-done = bf16[2048,256]{1,0:T(8,128)(2,1)} async-done(((bf16[256,256]{1,0:T(8,128)(2,1)}), bf16[2048,256]{1,0:T(8,128)(2,1)}) %all-gather.5.cloned.1.call-update) | async-done | bytes 1048592 | tf_op jit(solution)/shard_map/all_gather | solution.py:120
  93.0 2.3 copy.32
  95.3 7.0 %while.18 = (s32[]{:T(128)}, f32[2,2,256]{2,1,0:T(2,128)S(1)}, f32[2,2,256]{2,1,0:T(2,128)S(1)}, f32[256,2,2,128]{0,3,2,1:T(8,128)S(1)}, s32[]{:T(128)}, /*index...) while((s32[]{:T(128)}, f32[2,2,256]{2,1,0:T(2,128)S(1)}, ...), condition=%wide.region_5.6_spmd.clone, body=%wide.region_0.5_spmd.clone.sunk | while | flops 555225344 | bytes 20357496 | solution.py:56
  96.0 5.7 %conditional.3 = ((f32[2,2,256]{2,1,0:T(2,128)S(1)}, f32[2,2,256]{2,1,0:T(2,128)S(1)}, f32[256,2,2,128]{0,3,2,1:T(8,128)S(1)})) conditional(s32[]{:T(128)} %convert_element_type.127, (f32[2,2,256]{2,1,0:T(2,128)S(1)}, f32[2,2,256]{2,1,0:T(2,128)S(1)}, f32[256,2,2,128]{0,3,2,1:T(8,128)S(1)}) %tuple.46, (s32[]{:T(128)}, s32[]{:T(128)}, ...), branch_computations={%region_1.0_spmd, %region_2.4_spmd} | conditional | flops 555225344 | bytes 20356210 | solution.py:54
  96.3 2.3 fusion.5
  98.6 1.6 fusion.12
  100.2 1.4 fusion.4
  102.4 1.7 convolution_convert_fusion.1
  104.5 0.6 reduce-window.6
  105.7 1.4 scatter_custom_fusion
  107.1 26.4 %reduce-scatter.2.cloned.1.call-done = bf16[64,2048]{1,0:T(8,128)(2,1)} async-done(((bf16[256,2048]{1,0:T(8,128)(2,1)}), bf16[64,2048]{1,0:T(8,128)(2,1)}) %reduce-scatter.2.cloned.1.call-update) | async-done | bytes 262160 | tf_op jit(solution)/shard_map/reduce_scatter | solution.py:126
  133.5 1.0 add_convert_fusion
  134.9 3.3 %gather_fusion = bf16[512,2048]{1,0:T(8,128)(2,1)} fusion(bf16[65,2048]{1,0:T(8,128)(2,1)S(1)} %concatenate.3, s32[1024]{0:T(1024)S(1)} %pad_clamp_fusion.1), kind=kCustom, calls=%fused_computation | custom fusion | bytes 4196352 | tf_op jit(solution)/shard_map/gather | solution.py:155
  138.2 53.7 %all_to_all.10 = bf16[8,1,64,2048]{3,2,1,0:T(8,128)(2,1)S(1)} all-to-all(bf16[8,1,64,2048]{3,2,1,0:T(8,128)(2,1)} %bitcast.136), channel_id=1, replica_groups=mesh['sp'=8,'tp'=4] {'sp'}, dimensions={0} | all-to-all | bytes 4194304 | tf_op jit(solution)/shard_map/all_to_all | solution.py:156
  192.0 1.3 copy-done.1
  193.2 1.2 fusion.35
  194.5 6.2 %fusion.25 = bf16[8,1,64,2048]{3,2,1,0:T(8,128)(2,1)} fusion(bf16[1,384,2048]{2,1,0:T(8,128)(2,1)} %param.30, bf16[1,2048,384]{2,1,0:T(8,128)(2,1)} %param.29, bf16[8,1,64,2048]{3,2,1,0:T(8,128)(2,1)} %copy-done.1, f32[8,1,64,384]{3,2,0,1:T(8,128)S(1)} %fusion.35), kind=kOutput, calls=%fused_computation.31 | convolution fusion | flops 1612840960 | bytes 8126464 | tf_op jit(solution)/shard_map/necf,efd->necd/dot_general | solution.py:162
  200.7 4.7 %all-to-all-start.1 = ((bf16[8,1,64,2048]{3,2,1,0:T(8,128)(2,1)}), bf16[8,1,64,2048]{3,2,1,0:T(8,128)(2,1)}, u32[]{:S(2)}, u32[]{:S(2)}) async-start(bf16[8,1,64,2048]{3,2,1,0:T(8,128)(2,1)} %fusion.25), calls=%async_computation.2 | async-start | bytes 4194304 | tf_op jit(solution)/shard_map/all_to_all | solution.py:165
  205.6 1.8 fusion.85
  207.4 45.2 %all-to-all-done.1 = bf16[8,1,64,2048]{3,2,1,0:T(8,128)(2,1)} async-done(((bf16[8,1,64,2048]{3,2,1,0:T(8,128)(2,1)}), bf16[8,1,64,2048]{3,2,1,0:T(8,128)(2,1)}, u32[]{:S(2)}, u32[]{:S(2)}) %all-to-all-start.1) | async-done | bytes 2097184 | tf_op jit(solution)/shard_map/all_to_all | solution.py:165
  252.6 4.2 %gather_fusion.1 = bf16[256,2048]{1,0:T(8,128)(2,1)S(1)} fusion(bf16[512,2048]{1,0:T(8,128)(2,1)} %bitcast.41, s32[1024]{0:T(1024)S(1)} %pad_clamp_fusion), kind=kCustom, calls=%fused_computation.1 | custom fusion | bytes 2098176 | tf_op jit(solution)/shard_map/gather | solution.py:167
  256.8 1.7 reshape.128
  258.5 3.2 %multiply_reduce_fusion = f32[64,2048]{1,0:T(8,128)S(1)} fusion(f32[64,4,2048]{2,1,0:T(4,128)} %reshape.128, f32[64,4]{1,0:T(8,128)S(1)} %copy.35), kind=kLoop, calls=%fused_computation.40 | loop fusion | flops 917504 | bytes 2622464 | tf_op jit(solution)/shard_map/reduce_sum | solution.py:169
  261.7 3.4 %fusion.27 = bf16[64,2048]{1,0:T(8,128)(2,1)} fusion(f32[64,2048]{1,0:T(8,128)S(1)} %multiply_reduce_fusion, bf16[384,2048]{1,0:T(8,128)(2,1)} %param.33, bf16[2048,384]{1,0:T(8,128)(2,1)} %param.32, bf16[64,2048]{1,0:T(8,128)(2,1)S(1)} %add_convert_fusion, f32[64,384]{1,0:T(8,128)S(1)} %fusion.85, f32[2048]{0:T(1024)S(1)} %copy-done.4, ...), kind=kOutput, calls=%fused_computation.35 | convolution fusion | flops 202522624 | bytes 4301056 | tf_op jit(solution)/shard_map/dot_general | solution.py:174
  (60 shorter events, 2.1 us)
Async XLA Ops:
  6.5 95.8 %copy-start = (bf16[512,2048]{1,0:T(8,128)(2,1)S(1)}, bf16[512,2048]{1,0:T(8,128)(2,1)}, u32[]{:S(2)}) copy-start(bf16[512,2048]{1,0:T(8,128)(2,1)} %param.24) | copy-start | bytes 6291460
  6.5 45.0 %all-gather.3.cloned.1.call-start = ((), (), s32[]{:S(2)}) async-start(), calls=%async_computation.3 | async-start | bytes 1179648 | tf_op jit(solution)/shard_map/all_gather | solution.py:119
  8.4 84.6 %all-gather.5.cloned.1.call-start = ((), (), s32[]{:S(2)}) async-start(), calls=%async_computation.4 | async-start | bytes 1179648 | tf_op jit(solution)/shard_map/all_gather | solution.py:120
  9.1 124.4 %reduce-scatter.2.cloned.1.call-start = ((), (), s32[]{:S(2)}) async-start(), calls=%async_computation.5 | async-start | bytes 1310720 | tf_op jit(solution)/shard_map/reduce_scatter | solution.py:126
  96.2 2.4 copy-start.2
  102.4 1.8 copy-start.5
  102.4 31.1 %copy-start.3 = (bf16[64,2048]{1,0:T(8,128)(2,1)S(1)}, bf16[64,2048]{1,0:T(8,128)(2,1)}, u32[]{:S(2)}) copy-start(bf16[64,2048]{1,0:T(8,128)(2,1)} %param.19) | copy-start | bytes 786436
  102.4 32.3 %copy-start.4 = (f32[2048]{0:T(1024)S(1)}, f32[2048]{0:T(1024)}, u32[]{:S(2)}) copy-start(f32[2048]{0:T(1024)} %param.25) | copy-start | bytes 24580
  138.2 55.0 %copy-start.7 = (bf16[1,2048,384]{2,1,0:T(8,128)(2,1)S(1)}, bf16[1,2048,384]{2,1,0:T(8,128)(2,1)}, u32[]{:S(2)}) copy-start(bf16[1,2048,384]{2,1,0:T(8,128)(2,1)} %param.28) | copy-start | bytes 4718596
  191.9 1.3 copy-start.1
  200.7 4.7 %copy-start.6 = (f32[64,4]{0,1:T(4,128)S(1)}, f32[64,4]{0,1:T(4,128)}, u32[]{:S(2)}) copy-start(f32[64,4]{0,1:T(4,128)} %param.27) | copy-start | bytes 3076
  200.7 51.8 %all-to-all-start.1 = ((bf16[8,1,64,2048]{3,2,1,0:T(8,128)(2,1)}), bf16[8,1,64,2048]{3,2,1,0:T(8,128)(2,1)}, u32[]{:S(2)}, u32[]{:S(2)}) async-start(bf16[8,1,64,2048]{3,2,1,0:T(8,128)(2,1)} %fusion.25), calls=%async_computation.2 | async-start | bytes 4194304 | tf_op jit(solution)/shard_map/all_to_all | solution.py:165
Sparse Core Ops, SparseCore 0:
  9.4 42.1 all-gather.2
  53.7 39.2 all-gather.4
  104.3 29.1 reduce-scatter.1
where the time goes:
time: 272 us
  waiting for transfers between devices  118 us (43%)
  blocking collectives  86.7 us (32%)
  local copies, waits for them, and re-layouts  21.9 us (8%)
  matrix products  18.4 us (7%)
  between operations  13.3 us (5%)
  other arithmetic  6.9 us (3%)
  starting transfers between devices  4.77 us (2%)
    all_to_all x1, blocking collectives, local(): lax.all_to_all(outgoing, 'sp', split_axis=0, concat_axis=0, tiled=True)  53.7 us
    all_to_all x1, waiting for transfers between devices, local(): lax.all_to_all(processed, 'sp', split_axis=0, concat_axis=0, tiled=True)  45.2 us
    all_gather x1, waiting for transfers between devices, local(): lax.all_gather(value_rows, 'sp', axis=0, tiled=True)  39.2 us
    all_gather x1, blocking collectives, local(): all_sums = lax.all_gather(forget_sums, 'sp', axis=0, tiled=True)  33 us
    reduce_scatter x1, waiting for transfers between devices, local(): lax.psum_scatter(jnp.dot(attended, out_weight, preferred_element_type=jnp...  26.4 us
    unnamed x19, local copies, waits for them, and re-layouts  6.76 us
    all_gather x1, waiting for transfers between devices, local(): lax.all_gather(key_rows, 'sp', axis=0, tiled=True)  6.72 us
    dot_general x1, matrix products, local(): jnp.einsum('necf,efd->necd', hidden, expert_down, preferred_element_type=...  6.24 us
  transfers between devices with their start and end apart: 4, of which 4 were waited for; matrix products, arithmetic and copies ran while one was open for 4% of the time, Pallas kernels for 0%

commit v1 on v0

--- a/solution.py
+++ b/solution.py
@@ -86,7 +86,12 @@
     group_size = HEADS // KV_HEADS
     score_scale = HEAD_DIM ** (-0.5)
     own_first = sp_index * local_rows
-    all_sums = lax.all_gather(forget_sums, "sp", axis=0, tiled=True)
+    ring = [forget_sums]
+    for hop in range(7):
+        ring.append(lax.ppermute(ring[-1], "sp", [(dev, (dev + 1) % 8) for dev in range(8)]))
+    all_sums = jnp.roll(
+        jnp.concatenate(ring[::-1], axis=0), (lax.axis_index("sp") + 1) * ring[0].shape[0], axis=0
+    )
     positions = own_first + jnp.arange(local_rows, dtype=jnp.int32)
     groups = [
         (

time: 272 us -> 273 us (level)
  blocking collectives: 86.7 us -> 53.7 us
  waiting for transfers between devices: 118 us -> 147 us
  starting transfers between devices: 4.77 us -> 7.85 us
    ppermute x0 -> x7, waiting for transfers between devices: none -> 40.2 us  [local(): lax.ppermute(ring[-1], 'sp', [(dev, (dev + 1) % 8) for dev in range(8)])]
    all_gather x1 -> x0, blocking collectives: 33 us -> none  [local(): all_sums = lax.all_gather(forget_sums, 'sp', axis=0, tiled=True)]
    all_gather x1, waiting for transfers between devices: 6.72 us -> 0.02 us  [local(): lax.all_gather(key_rows, 'sp', axis=0, tiled=True)]
    all_gather x1, waiting for transfers between devices: 39.2 us -> 34.8 us  [local(): lax.all_gather(value_rows, 'sp', axis=0, tiled=True)]
    ppermute x0 -> x7, starting transfers between devices: none -> 3.06 us  [local(): lax.ppermute(ring[-1], 'sp', [(dev, (dev + 1) % 8) for dev in range(8)])]
    unnamed x19 -> x34, local copies, waits for them, and re-layouts: 6.76 us -> 7.58 us
  transfers between devices with their start and end apart: 4 -> 11, of which waited for: 4 -> 10; matrix products, arithmetic and copies ran while one was open for 4% -> 4% of each run, Pallas kernels for 0% -> 0%
where the time goes in v1:
time: 273 us; the launch traced here: 272 us
  waiting for transfers between devices  147 us (54%)
  blocking collectives  53.7 us (20%)
  local copies, waits for them, and re-layouts  23.5 us (9%)
  matrix products  18.4 us (7%)
  between operations  13.4 us (5%)
  starting transfers between devices  7.85 us (3%)
  other arithmetic  6.9 us (3%)
    all_to_all x1, blocking collectives, local(): lax.all_to_all(outgoing, 'sp', split_axis=0, concat_axis=0, tiled=True)  53.7 us
    all_to_all x1, waiting for transfers between devices, local(): lax.all_to_all(processed, 'sp', split_axis=0, concat_axis=0, tiled=True)  45.2 us
    ppermute x7, waiting for transfers between devices, local(): lax.ppermute(ring[-1], 'sp', [(dev, (dev + 1) % 8) for dev in range(8)])  40.2 us
    all_gather x1, waiting for transfers between devices, local(): lax.all_gather(value_rows, 'sp', axis=0, tiled=True)  34.8 us
    reduce_scatter x1, waiting for transfers between devices, local(): lax.psum_scatter(jnp.dot(attended, out_weight, preferred_element_type=jnp...  26.4 us
    unnamed x34, local copies, waits for them, and re-layouts  7.58 us
    dot_general x1, matrix products, local(): jnp.einsum('necf,efd->necd', hidden, expert_down, preferred_element_type=...  6.24 us
  transfers between devices with their start and end apart: 11, of which 10 were waited for; matrix products, arithmetic and copies ran while one was open for 4% of the time, Pallas kernels for 0%

profile of v1, /device:TPU:0, one launch (start us, length us, event | category | flops | bytes accessed | tf_op | source)
XLA Modules:
  0.0 271.9 jit_solution(6082530103357456302)
XLA Ops:
  6.5 1.8 copy.30
  8.4 3.0 %collective-permute-start = (f32[256,4]{0,1:T(4,128)}, f32[256,4]{0,1:T(4,128)S(1)}, u32[]{:S(2)}, u32[]{:S(2)}) collective-permute-start(f32[256,4]{0,1:T(4,128)} %param.23), channel_id=1, source_target_pairs={{0,4},{4,8},{8,12},{12,16},{16,20},{20,24},{24,28},{28,0},{1,5},{5... | collective-permute-start | bytes 12296 | tf_op jit(solution)/shard_map/ppermute | solution.py:91
  11.5 4.8 %collective-permute-done = f32[256,4]{0,1:T(4,128)S(1)} collective-permute-done((f32[256,4]{0,1:T(4,128)}, f32[256,4]{0,1:T(4,128)S(1)}, u32[]{:S(2)}, u32[]{:S(2)}) %collective-permute-start) | collective-permute-done | bytes 4128 | tf_op jit(solution)/shard_map/ppermute | solution.py:91
  16.3 6.3 %collective-permute-done.1 = f32[256,4]{0,1:T(4,128)S(1)} collective-permute-done((f32[256,4]{0,1:T(4,128)S(1)}, f32[256,4]{0,1:T(4,128)S(1)}, u32[]{:S(2)}, u32[]{:S(2)}) %collective-permute-start.1) | collective-permute-done | bytes 4128 | tf_op jit(solution)/shard_map/ppermute | solution.py:91
  22.6 6.3 %collective-permute-done.2 = f32[256,4]{0,1:T(4,128)S(1)} collective-permute-done((f32[256,4]{0,1:T(4,128)S(1)}, f32[256,4]{0,1:T(4,128)S(1)}, u32[]{:S(2)}, u32[]{:S(2)}) %collective-permute-start.2) | collective-permute-done | bytes 4128 | tf_op jit(solution)/shard_map/ppermute | solution.py:91
  28.9 6.3 %collective-permute-done.3 = f32[256,4]{0,1:T(4,128)S(1)} collective-permute-done((f32[256,4]{0,1:T(4,128)S(1)}, f32[256,4]{0,1:T(4,128)S(1)}, u32[]{:S(2)}, u32[]{:S(2)}) %collective-permute-start.3) | collective-permute-done | bytes 4128 | tf_op jit(solution)/shard_map/ppermute | solution.py:91
  35.2 6.4 %collective-permute-done.4 = f32[256,4]{0,1:T(4,128)S(1)} collective-permute-done((f32[256,4]{0,1:T(4,128)S(1)}, f32[256,4]{0,1:T(4,128)S(1)}, u32[]{:S(2)}, u32[]{:S(2)}) %collective-permute-start.4) | collective-permute-done | bytes 4128 | tf_op jit(solution)/shard_map/ppermute | solution.py:91
  41.7 6.4 %collective-permute-done.5 = f32[256,4]{0,1:T(4,128)S(1)} collective-permute-done((f32[256,4]{0,1:T(4,128)S(1)}, f32[256,4]{0,1:T(4,128)S(1)}, u32[]{:S(2)}, u32[]{:S(2)}) %collective-permute-start.5) | collective-permute-done | bytes 4128 | tf_op jit(solution)/shard_map/ppermute | solution.py:91
  50.7 3.7 %collective-permute-done.6 = f32[256,4]{0,1:T(4,128)S(1)} collective-permute-done((f32[256,4]{0,1:T(4,128)S(1)}, f32[256,4]{0,1:T(4,128)S(1)}, u32[]{:S(2)}, u32[]{:S(2)}) %collective-permute-start.6) | collective-permute-done | bytes 4128 | tf_op jit(solution)/shard_map/ppermute | solution.py:91
  56.0 2.3 copy.33
  58.2 34.8 %all-gather.5.cloned.1.call-done = bf16[2048,256]{1,0:T(8,128)(2,1)} async-done(((bf16[256,256]{1,0:T(8,128)(2,1)}), bf16[2048,256]{1,0:T(8,128)(2,1)}) %all-gather.5.cloned.1.call-update) | async-done | bytes 1048592 | tf_op jit(solution)/shard_map/all_gather | solution.py:125
  93.1 2.3 copy.32
  95.4 7.1 %while.18 = (s32[]{:T(128)}, f32[2,2,256]{2,1,0:T(2,128)S(1)}, f32[2,2,256]{2,1,0:T(2,128)S(1)}, f32[256,2,2,128]{0,3,2,1:T(8,128)S(1)}, s32[]{:T(128)}, /*index...) while((s32[]{:T(128)}, f32[2,2,256]{2,1,0:T(2,128)S(1)}, ...), condition=%wide.region_5.6_spmd.clone, body=%wide.region_0.5_spmd.clone.sunk | while | flops 555225344 | bytes 20357496 | solution.py:56
  96.1 5.7 %conditional.3 = ((f32[2,2,256]{2,1,0:T(2,128)S(1)}, f32[2,2,256]{2,1,0:T(2,128)S(1)}, f32[256,2,2,128]{0,3,2,1:T(8,128)S(1)})) conditional(s32[]{:T(128)} %convert_element_type.127, (f32[2,2,256]{2,1,0:T(2,128)S(1)}, f32[2,2,256]{2,1,0:T(2,128)S(1)}, f32[256,2,2,128]{0,3,2,1:T(8,128)S(1)}) %tuple.46, (s32[]{:T(128)}, s32[]{:T(128)}, ...), branch_computations={%region_1.1_spmd, %region_2.4_spmd} | conditional | flops 555225344 | bytes 20356210 | solution.py:54
  96.4 2.3 fusion.5
  98.8 1.6 fusion.12
  100.4 1.4 fusion.4
  102.7 1.7 convolution_convert_fusion.1
  105.9 1.4 scatter_custom_fusion
  107.4 26.4 %reduce-scatter.2.cloned.1.call-done = bf16[64,2048]{1,0:T(8,128)(2,1)} async-done(((bf16[256,2048]{1,0:T(8,128)(2,1)}), bf16[64,2048]{1,0:T(8,128)(2,1)}) %reduce-scatter.2.cloned.1.call-update) | async-done | bytes 262160 | tf_op jit(solution)/shard_map/reduce_scatter | solution.py:131
  135.1 3.3 %gather_fusion = bf16[512,2048]{1,0:T(8,128)(2,1)} fusion(bf16[65,2048]{1,0:T(8,128)(2,1)S(1)} %concatenate.10, s32[1024]{0:T(1024)S(1)} %pad_clamp_fusion.1), kind=kCustom, calls=%fused_computation | custom fusion | bytes 4196352 | tf_op jit(solution)/shard_map/gather | solution.py:160
  138.4 53.7 %all_to_all.10 = bf16[8,1,64,2048]{3,2,1,0:T(8,128)(2,1)S(1)} all-to-all(bf16[8,1,64,2048]{3,2,1,0:T(8,128)(2,1)} %bitcast.136), channel_id=1, replica_groups=mesh['sp'=8,'tp'=4] {'sp'}, dimensions={0} | all-to-all | bytes 4194304 | tf_op jit(solution)/shard_map/all_to_all | solution.py:161
  192.1 1.3 copy-done.1
  193.5 1.2 fusion.35
  194.7 6.2 %fusion.25 = bf16[8,1,64,2048]{3,2,1,0:T(8,128)(2,1)} fusion(bf16[1,384,2048]{2,1,0:T(8,128)(2,1)} %param.30, bf16[1,2048,384]{2,1,0:T(8,128)(2,1)} %param.29, bf16[8,1,64,2048]{3,2,1,0:T(8,128)(2,1)} %copy-done.1, f32[8,1,64,384]{3,2,0,1:T(8,128)S(1)} %fusion.35), kind=kOutput, calls=%fused_computation.31 | convolution fusion | flops 1612840960 | bytes 8126464 | tf_op jit(solution)/shard_map/necf,efd->necd/dot_general | solution.py:167
  200.9 4.7 %all-to-all-start.1 = ((bf16[8,1,64,2048]{3,2,1,0:T(8,128)(2,1)}), bf16[8,1,64,2048]{3,2,1,0:T(8,128)(2,1)}, u32[]{:S(2)}, u32[]{:S(2)}) async-start(bf16[8,1,64,2048]{3,2,1,0:T(8,128)(2,1)} %fusion.25), calls=%async_computation.2 | async-start | bytes 4194304 | tf_op jit(solution)/shard_map/all_to_all | solution.py:170
  205.8 1.8 fusion.85
  207.6 45.2 %all-to-all-done.1 = bf16[8,1,64,2048]{3,2,1,0:T(8,128)(2,1)} async-done(((bf16[8,1,64,2048]{3,2,1,0:T(8,128)(2,1)}), bf16[8,1,64,2048]{3,2,1,0:T(8,128)(2,1)}, u32[]{:S(2)}, u32[]{:S(2)}) %all-to-all-start.1) | async-done | bytes 2097184 | tf_op jit(solution)/shard_map/all_to_all | solution.py:170
  252.8 4.2 %gather_fusion.1 = bf16[256,2048]{1,0:T(8,128)(2,1)S(1)} fusion(bf16[512,2048]{1,0:T(8,128)(2,1)} %bitcast.41, s32[1024]{0:T(1024)S(1)} %pad_clamp_fusion), kind=kCustom, calls=%fused_computation.1 | custom fusion | bytes 2098176 | tf_op jit(solution)/shard_map/gather | solution.py:172
  257.0 1.7 reshape.128
  258.8 3.2 %multiply_reduce_fusion = f32[64,2048]{1,0:T(8,128)S(1)} fusion(f32[64,4,2048]{2,1,0:T(4,128)} %reshape.128, f32[64,4]{1,0:T(8,128)S(1)} %copy.35), kind=kLoop, calls=%fused_computation.40 | loop fusion | flops 917504 | bytes 2622464 | tf_op jit(solution)/shard_map/reduce_sum | solution.py:174
  261.9 3.4 %fusion.27 = bf16[64,2048]{1,0:T(8,128)(2,1)} fusion(f32[64,2048]{1,0:T(8,128)S(1)} %multiply_reduce_fusion, bf16[384,2048]{1,0:T(8,128)(2,1)} %param.33, bf16[2048,384]{1,0:T(8,128)(2,1)} %param.32, bf16[64,2048]{1,0:T(8,128)(2,1)S(1)} %add_convert_fusion, f32[64,384]{1,0:T(8,128)S(1)} %fusion.85, f32[2048]{0:T(1024)S(1)} %copy-done.4, ...), kind=kOutput, calls=%fused_computation.35 | convolution fusion | flops 202522624 | bytes 4301056 | tf_op jit(solution)/shard_map/dot_general | solution.py:179
  (90 shorter events, 7.7 us)
Async XLA Ops:
  6.5 96.1 %copy-start = (bf16[512,2048]{1,0:T(8,128)(2,1)S(1)}, bf16[512,2048]{1,0:T(8,128)(2,1)}, u32[]{:S(2)}) copy-start(bf16[512,2048]{1,0:T(8,128)(2,1)} %param.24) | copy-start | bytes 6291460
  6.5 49.4 %all-gather.3.cloned.1.call-start = ((), (), s32[]{:S(2)}) async-start(), calls=%async_computation.3 | async-start | bytes 1179648 | tf_op jit(solution)/shard_map/all_gather | solution.py:124
  8.4 84.7 %all-gather.5.cloned.1.call-start = ((), (), s32[]{:S(2)}) async-start(), calls=%async_computation.4 | async-start | bytes 1179648 | tf_op jit(solution)/shard_map/all_gather | solution.py:125
  8.4 7.9 %collective-permute-start = (f32[256,4]{0,1:T(4,128)}, f32[256,4]{0,1:T(4,128)S(1)}, u32[]{:S(2)}, u32[]{:S(2)}) collective-permute-start(f32[256,4]{0,1:T(4,128)} %param.23), channel_id=1, source_target_pairs={{0,4},{4,8},{8,12},{12,16},{16,20},{20,24},{24,28},{28,0},{1,5},{5... | collective-permute-start | bytes 12296 | tf_op jit(solution)/shard_map/ppermute | solution.py:91
  16.3 6.3 %collective-permute-start.1 = (f32[256,4]{0,1:T(4,128)S(1)}, f32[256,4]{0,1:T(4,128)S(1)}, u32[]{:S(2)}, u32[]{:S(2)}) collective-permute-start(f32[256,4]{0,1:T(4,128)S(1)} %collective-permute-done), channel_id=1, source_target_pairs={{0,4},{4,8},{8,12},{12,16},{16,20},{20,24},{24,28},{28,0},{1,5},{5... | collective-permute-start | bytes 12296 | tf_op jit(solution)/shard_map/ppermute | solution.py:91
  22.6 6.3 %collective-permute-start.2 = (f32[256,4]{0,1:T(4,128)S(1)}, f32[256,4]{0,1:T(4,128)S(1)}, u32[]{:S(2)}, u32[]{:S(2)}) collective-permute-start(f32[256,4]{0,1:T(4,128)S(1)} %collective-permute-done.1), channel_id=1, source_target_pairs={{0,4},{4,8},{8,12},{12,16},{16,20},{20,24},{24,28},{28,0},{1,5},{5... | collective-permute-start | bytes 12296 | tf_op jit(solution)/shard_map/ppermute | solution.py:91
  28.9 6.3 %collective-permute-start.3 = (f32[256,4]{0,1:T(4,128)S(1)}, f32[256,4]{0,1:T(4,128)S(1)}, u32[]{:S(2)}, u32[]{:S(2)}) collective-permute-start(f32[256,4]{0,1:T(4,128)S(1)} %collective-permute-done.2), channel_id=1, source_target_pairs={{0,4},{4,8},{8,12},{12,16},{16,20},{20,24},{24,28},{28,0},{1,5},{5... | collective-permute-start | bytes 12296 | tf_op jit(solution)/shard_map/ppermute | solution.py:91
  35.2 6.4 %collective-permute-start.4 = (f32[256,4]{0,1:T(4,128)S(1)}, f32[256,4]{0,1:T(4,128)S(1)}, u32[]{:S(2)}, u32[]{:S(2)}) collective-permute-start(f32[256,4]{0,1:T(4,128)S(1)} %collective-permute-done.3), channel_id=1, source_target_pairs={{0,4},{4,8},{8,12},{12,16},{16,20},{20,24},{24,28},{28,0},{1,5},{5... | collective-permute-start | bytes 12296 | tf_op jit(solution)/shard_map/ppermute | solution.py:91
  41.6 6.4 %collective-permute-start.5 = (f32[256,4]{0,1:T(4,128)S(1)}, f32[256,4]{0,1:T(4,128)S(1)}, u32[]{:S(2)}, u32[]{:S(2)}) collective-permute-start(f32[256,4]{0,1:T(4,128)S(1)} %collective-permute-done.4), channel_id=1, source_target_pairs={{0,4},{4,8},{8,12},{12,16},{16,20},{20,24},{24,28},{28,0},{1,5},{5... | collective-permute-start | bytes 12296 | tf_op jit(solution)/shard_map/ppermute | solution.py:91
  41.7 92.1 %reduce-scatter.2.cloned.1.call-start = ((), (), s32[]{:S(2)}) async-start(), calls=%async_computation.5 | async-start | bytes 1310720 | tf_op jit(solution)/shard_map/reduce_scatter | solution.py:131
  48.1 6.3 %collective-permute-start.6 = (f32[256,4]{0,1:T(4,128)S(1)}, f32[256,4]{0,1:T(4,128)S(1)}, u32[]{:S(2)}, u32[]{:S(2)}) collective-permute-start(f32[256,4]{0,1:T(4,128)S(1)} %collective-permute-done.5), channel_id=1, source_target_pairs={{0,4},{4,8},{8,12},{12,16},{16,20},{20,24},{24,28},{28,0},{1,5},{5... | collective-permute-start | bytes 12296 | tf_op jit(solution)/shard_map/ppermute | solution.py:91
  96.4 2.4 copy-start.2
  102.6 1.8 copy-start.5
  102.6 31.1 %copy-start.3 = (bf16[64,2048]{1,0:T(8,128)(2,1)S(1)}, bf16[64,2048]{1,0:T(8,128)(2,1)}, u32[]{:S(2)}) copy-start(bf16[64,2048]{1,0:T(8,128)(2,1)} %param.19) | copy-start | bytes 786436
  102.7 32.3 %copy-start.4 = (f32[2048]{0:T(1024)S(1)}, f32[2048]{0:T(1024)}, u32[]{:S(2)}) copy-start(f32[2048]{0:T(1024)} %param.25) | copy-start | bytes 24580
  138.4 55.0 %copy-start.7 = (bf16[1,2048,384]{2,1,0:T(8,128)(2,1)S(1)}, bf16[1,2048,384]{2,1,0:T(8,128)(2,1)}, u32[]{:S(2)}) copy-start(bf16[1,2048,384]{2,1,0:T(8,128)(2,1)} %param.28) | copy-start | bytes 4718596
  192.1 1.3 copy-start.1
  200.9 4.7 %copy-start.6 = (f32[64,4]{0,1:T(4,128)S(1)}, f32[64,4]{0,1:T(4,128)}, u32[]{:S(2)}) copy-start(f32[64,4]{0,1:T(4,128)} %param.27) | copy-start | bytes 3076
  200.9 51.9 %all-to-all-start.1 = ((bf16[8,1,64,2048]{3,2,1,0:T(8,128)(2,1)}), bf16[8,1,64,2048]{3,2,1,0:T(8,128)(2,1)}, u32[]{:S(2)}, u32[]{:S(2)}) async-start(bf16[8,1,64,2048]{3,2,1,0:T(8,128)(2,1)} %fusion.25), calls=%async_computation.2 | async-start | bytes 4194304 | tf_op jit(solution)/shard_map/all_to_all | solution.py:170
Sparse Core Ops, SparseCore 0:
  9.4 42.0 all-gather.2
  53.6 39.4 all-gather.4
  104.5 29.1 reduce-scatter.1
